TPU v7x, 32 devices: a whole 2x2x4 slice. The times are simulated.
32 devices in a mesh: grp: 2 (over x), ep: 16 (over z, y, core).
Axes of the slice: x: 2, y: 2, z: 4, core: 2. Of those that a mesh axis runs over, the one named last changes fastest.
Arguments:
- tokens: bfloat16 [16384, 2048], P(('grp', 'ep')), parts along dimension 0, may hold values from -6 to 6
- norm_gain: float32 [2048], replicated, may hold values from 0.1 to 1.9
- route_ids: int32 [16384, 2], P(('grp', 'ep')), parts along dimension 0, may hold values from 0 to 15, all different within a row; in each aligned block of 512 rows (0 to 511, 512 to 1023, ...) at most 96 rows name the same one
- route_gates: float32 [16384, 2], P(('grp', 'ep')), parts along dimension 0, may hold values from 0.05 to 1
- w_gate: bfloat16 [16, 2048, 1024], P('ep'), may hold values from -0.125 to 0.125
- w_up: bfloat16 [16, 2048, 1024], P('ep'), may hold values from -0.125 to 0.125
- w_down: bfloat16 [16, 1024, 2048], P('ep'), may hold values from -0.1875 to 0.1875
Outputs:
- mixed: bfloat16 [16384, 2048], P(('grp', 'ep')), parts along dimension 0
There are 2 independent parts, one for each index of `grp`. A program takes and returns all parts, laid end to end along the dimension named above; an argument that names none is the same for every part. Nothing has to cross between parts.
Inputs may be any that keep to these rules, and one draw needn't show every extreme that they name: `route_ids`: each row names 2 different experts. Among the rows of one device no expert is named more than 96 times, and in some devices' rows one expert is named exactly 96 times.
All inputs are finite; a program needn't handle non-finite values.
Results may differ from a plain program's by a relative error of at most 0.0071.
Values may be sent and summed in bfloat16 or wider, within the bound.
A program may use at most 128 MiB of HBM per device.

v0:
```python
import jax
import jax.numpy as jnp
from jax import lax
from jax.sharding import PartitionSpec as P

EPS = 1e-06


def rms_norm(tokens, norm_gain):
    floats = tokens.astype(jnp.float32)
    scale = lax.rsqrt(jnp.mean(floats * floats, axis=-1, keepdims=True) + EPS)
    return (floats * scale * norm_gain).astype(jnp.bfloat16)


def slot_index(route_ids, experts, capacity):
    flat_ids = route_ids.reshape(-1)
    onehot = (flat_ids[:, None] == jnp.arange(experts, dtype=jnp.int32)[None, :]).astype(jnp.int32)
    ranked = jnp.cumsum(onehot, axis=0) - onehot
    return flat_ids * capacity + jnp.sum(ranked * onehot, axis=1)


def expert_block(arrived, w_gate, w_up, w_down):
    gate_pre = jnp.einsum("sjcd,jdf->sjcf", arrived, w_gate, preferred_element_type=jnp.float32)
    up_pre = jnp.einsum("sjcd,jdf->sjcf", arrived, w_up, preferred_element_type=jnp.float32)
    hidden = (jax.nn.silu(gate_pre) * up_pre).astype(jnp.bfloat16)
    return jnp.einsum("sjcf,jfd->sjcd", hidden, w_down, preferred_element_type=jnp.float32).astype(
        jnp.bfloat16
    )


def body(tokens, norm_gain, route_ids, route_gates, w_gate, w_up, w_down):
    tok_rows, width = tokens.shape
    top_count = route_ids.shape[1]
    devices = lax.axis_size("ep")
    local_experts = w_gate.shape[0]
    experts = local_experts * devices
    capacity = 3 * tok_rows * top_count // (2 * experts)
    normed = rms_norm(tokens, norm_gain)
    weights = route_gates / jnp.sum(route_gates, axis=1, keepdims=True)
    places = slot_index(route_ids, experts, capacity)
    row_of = jnp.arange(tok_rows * top_count, dtype=jnp.int32) // top_count
    outgoing = jnp.zeros((experts * capacity, width), jnp.bfloat16).at[places].set(normed[row_of])
    outgoing = outgoing.reshape(devices, local_experts, capacity, width)
    finished = expert_block(
        lax.all_to_all(outgoing, "ep", split_axis=0, concat_axis=0, tiled=True),
        w_gate,
        w_up,
        w_down,
    )
    returned = lax.all_to_all(finished, "ep", split_axis=0, concat_axis=0, tiled=True)
    picked = returned.reshape(experts * capacity, width)[places]
    shaped = picked.astype(jnp.float32).reshape(tok_rows, top_count, width)
    return jnp.sum(shaped * weights[:, :, None], axis=1).astype(jnp.bfloat16)


def solution(mesh):
    placed = (
        P(("grp", "ep"), None),
        P(),
        P(("grp", "ep"), None),
        P(("grp", "ep"), None),
        P("ep", None, None),
        P("ep", None, None),
        P("ep", None, None),
    )
    return jax.shard_map(
        body, mesh=mesh, in_specs=placed, out_specs=P(("grp", "ep"), None), check_vma=False
    )
```

profile of v0, /device:TPU:15, one launch (start us, length us, event | category | flops | bytes accessed | tf_op | source)
XLA Modules:
  0.0 381.3 jit_solution(8459370248406404132)
XLA Ops:
  0.0 1.0 copy.18
  1.0 0.2 eq.29
  1.2 0.2 eq.25
  1.3 0.7 broadcast_multiply_fusion
  2.0 4.5 %reduce-window.6 = s32[16,8,128]{2,1,0:T(8,128)S(1)} reduce-window(s32[16,8,128]{2,1,0:T(8,128)S(1)} %fusion.25, s32[]{:T(128)} %constant.31.clone.1), window={size=1x1x128 pad=0_0x0_0x127_0}, to_apply=%region_0.0 | reduce-window | flops 2080768 | bytes 131076 | tf_op jit(solution)/shard_map/reduce-window
  6.6 0.1 slice.12
  6.6 0.1 copy.20
  6.8 0.1 copy.21
  6.9 0.1 broadcast_add_fusion
  7.0 0.1 copy.17
  7.1 0.2 mul.55
  7.3 2.1 fusion.8
  9.5 2.6 fusion.10
  12.0 22.0 %scatter_custom_fusion = bf16[1536,2048]{1,0:T(8,128)(2,1)} fusion(s32[1024]{0:T(1024)S(1)} %bitcast.84, bf16[512,2048]{1,0:T(8,128)(2,1)} %fusion.10, s32[1024]{0:T(1024)S(1)} %broadcast_clamp_fusion.1, bf16[]{:T(256)} %constant.29.clone.1), kind=kCustom, calls=%fused_computation.24 | custom fusion | bytes 6291968 | tf_op jit(solution)/shard_map/scatter | solution.py:42
  34.0 143.9 %all_to_all.10 = bf16[16,1,96,2048]{3,2,1,0:T(8,128)(2,1)S(1)} all-to-all(bf16[16,1,96,2048]{3,2,1,0:T(8,128)(2,1)} %bitcast.80), channel_id=1, replica_groups=mesh['grp'=2,'ep'=16] {'ep'}, dimensions={0} | all-to-all | bytes 12582912 | tf_op jit(solution)/shard_map/all_to_all | solution.py:45
  178.0 6.8 %fusion.4 = f32[16,96,1024]{2,1,0:T(8,128)S(1)} fusion(bf16[16,1,96,2048]{3,2,1,0:T(8,128)(2,1)S(1)} %all_to_all.10, bf16[1,2048,1024]{2,1,0:T(8,128)(2,1)S(1)} %copy-done.2), kind=kOutput, calls=%fused_computation.11 | convolution fusion | flops 6442450944 | bytes 16777216 | tf_op jit(solution)/shard_map/sjcd,jdf->sjcf/dot_general | solution.py:24
  184.8 7.7 %fusion = bf16[16,1,96,1024]{3,2,0,1:T(8,128)(2,1)S(1)} fusion(f32[16,96,1024]{2,1,0:T(8,128)S(1)} %fusion.4, bf16[1,2048,1024]{2,1,0:T(8,128)(2,1)S(1)} %copy-done.3, bf16[16,1,96,2048]{3,2,1,0:T(8,128)(2,1)S(1)} %all_to_all.10), kind=kOutput, calls=%fused_computation.5 | convolution fusion | flops 6451888128 | bytes 19922944 | tf_op jit(solution)/shard_map/sjcd,jdf->sjcf/dot_general | solution.py:23
  192.5 8.7 %convert_bitcast_fusion = bf16[16,1,96,2048]{3,2,1,0:T(8,128)(2,1)} fusion(bf16[1,1024,2048]{2,1,0:T(8,128)(2,1)S(1)} %copy-done.4, bf16[16,1,96,1024]{3,2,0,1:T(8,128)(2,1)S(1)} %fusion), kind=kOutput, calls=%fused_computation.15 | convolution fusion | flops 6445596672 | bytes 13631488 | tf_op jit(solution)/shard_map/sjcf,jfd->sjcd/dot_general | solution.py:26
  201.2 5.6 %all-to-all-start.1 = ((bf16[16,1,96,2048]{3,2,1,0:T(8,128)(2,1)}), bf16[16,1,96,2048]{3,2,1,0:T(8,128)(2,1)}, u32[]{:S(2)}, u32[]{:S(2)}) async-start(bf16[16,1,96,2048]{3,2,1,0:T(8,128)(2,1)} %convert_bitcast_fusion), calls=%async_computation.1 | async-start | bytes 12582912 | tf_op jit(solution)/shard_map/all_to_all | solution.py:50
  206.8 0.1 copy.23
  207.0 137.2 %all-to-all-done.1 = bf16[16,1,96,2048]{3,2,1,0:T(8,128)(2,1)} async-done(((bf16[16,1,96,2048]{3,2,1,0:T(8,128)(2,1)}), bf16[16,1,96,2048]{3,2,1,0:T(8,128)(2,1)}, u32[]{:S(2)}, u32[]{:S(2)}) %all-to-all-start.1) | async-done | bytes 6291488 | tf_op jit(solution)/shard_map/all_to_all | solution.py:50
  344.2 12.4 %gather_fusion = bf16[1024,2048]{1,0:T(8,128)(2,1)} fusion(bf16[1536,2048]{1,0:T(8,128)(2,1)} %bitcast.26, s32[1024]{0:T(1024)S(1)} %broadcast_clamp_fusion), kind=kCustom, calls=%fused_computation.1 | custom fusion | bytes 8392704 | tf_op jit(solution)/shard_map/gather | solution.py:51
  356.6 9.6 %reshape.138 = f32[512,2,2048]{2,1,0:T(2,128)} reshape(bf16[1024,2048]{1,0:T(8,128)(2,1)} %gather_fusion) | data formatting | bytes 12582912 | tf_op jit(solution)/shard_map/convert_element_type | solution.py:52
  366.2 15.0 %multiply_reduce_fusion = bf16[512,2048]{1,0:T(8,128)(2,1)} fusion(f32[512,2,2048]{2,1,0:T(2,128)} %reshape.138, f32[512,2]{1,0:T(8,128)S(1)} %copy.23), kind=kLoop, calls=%fused_computation.3 | loop fusion | flops 3145728 | bytes 10489856 | tf_op jit(solution)/shard_map/reduce_sum | solution.py:53
  (21 shorter events, 0.2 us)
Async XLA Ops:
  0.0 9.5 %copy-start = (bf16[512,2048]{1,0:T(8,128)(2,1)S(1)}, bf16[512,2048]{1,0:T(8,128)(2,1)}, u32[]{:S(2)}) copy-start(bf16[512,2048]{1,0:T(8,128)(2,1)} %param.7) | copy-start | bytes 6291460
  34.0 143.9 %copy-start.2 = (bf16[1,2048,1024]{2,1,0:T(8,128)(2,1)S(1)}, bf16[1,2048,1024]{2,1,0:T(8,128)(2,1)}, u32[]{:S(2)}) copy-start(bf16[1,2048,1024]{2,1,0:T(8,128)(2,1)} %param.12) | copy-start | bytes 12582916
  178.0 6.8 %copy-start.3 = (bf16[1,2048,1024]{2,1,0:T(8,128)(2,1)S(1)}, bf16[1,2048,1024]{2,1,0:T(8,128)(2,1)}, u32[]{:S(2)}) copy-start(bf16[1,2048,1024]{2,1,0:T(8,128)(2,1)} %param.11) | copy-start | bytes 12582916
  184.8 7.7 %copy-start.4 = (bf16[1,1024,2048]{2,1,0:T(8,128)(2,1)S(1)}, bf16[1,1024,2048]{2,1,0:T(8,128)(2,1)}, u32[]{:S(2)}) copy-start(bf16[1,1024,2048]{2,1,0:T(8,128)(2,1)} %param.13) | copy-start | bytes 12582916
  201.2 5.6 %copy-start.1 = (f32[512,2]{0,1:T(2,128)S(1)}, f32[512,2]{0,1:T(2,128)}, u32[]{:S(2)}) copy-start(f32[512,2]{0,1:T(2,128)} %param.10) | copy-start | bytes 12292
  201.2 143.0 %all-to-all-start.1 = ((bf16[16,1,96,2048]{3,2,1,0:T(8,128)(2,1)}), bf16[16,1,96,2048]{3,2,1,0:T(8,128)(2,1)}, u32[]{:S(2)}, u32[]{:S(2)}) async-start(bf16[16,1,96,2048]{3,2,1,0:T(8,128)(2,1)} %convert_bitcast_fusion), calls=%async_computation.1 | async-start | bytes 12582912 | tf_op jit(solution)/shard_map/all_to_all | solution.py:50
where the time goes:
time: 382 us; the launch traced here: 381 us
  blocking collectives  144 us (38%)
  waiting for transfers between devices  137 us (36%)
  local copies, waits for them, and re-layouts  46.1 us (12%)
  other arithmetic  25.1 us (7%)
  matrix products  23.2 us (6%)
  starting transfers between devices  5.55 us (1%)
    all_to_all x1, blocking collectives, body(): lax.all_to_all(outgoing, 'ep', split_axis=0, concat_axis=0, tiled=True)  144 us
    all_to_all x1, waiting for transfers between devices, body(): lax.all_to_all(finished, 'ep', split_axis=0, concat_axis=0, tiled=True)  137 us
    scatter x1, local copies, waits for them, and re-layouts, body(): jnp.zeros((experts * capacity, width), jnp.bfloat16).at[places]  22 us
    reduce_sum x1, other arithmetic, body(): return jnp.sum(shaped * weights[:, :, None], axis=1).astype(jnp.bfloat16)  15 us
    gather x1, local copies, waits for them, and re-layouts, body(): picked = returned.reshape(experts * capacity, width)[places]  12.4 us
    convert_element_type x1, local copies, waits for them, and re-layouts, body(): shaped = picked.astype(jnp.float32).reshape(tok_rows, top_count, width)  9.65 us
    dot_general x1, matrix products, expert_block(): jnp.einsum('sjcf,jfd->sjcd', hidden, w_down, preferred_element_type=jnp.f...  8.7 us
    dot_general x1, matrix products, expert_block(): jnp.einsum('sjcd,jdf->sjcf', arrived, w_gate, preferred_element_type=jnp....  7.71 us
  transfers between devices with their start and end apart: 1, of which 1 were waited for; matrix products, arithmetic and copies ran while one was open for 0% of the time, Pallas kernels for 0%

commit v1 on v0

v1 whole, which is shorter than its diff:
```python
import jax
import jax.numpy as jnp
from jax import lax
from jax.sharding import PartitionSpec as P

EPS = 1e-06
CHUNKS = 2


def rms_norm(tokens, norm_gain):
    floats = tokens.astype(jnp.float32)
    scale = lax.rsqrt(jnp.mean(floats * floats, axis=-1, keepdims=True) + EPS)
    return (floats * scale * norm_gain).astype(jnp.bfloat16)


def slot_index(route_ids, experts, capacity):
    rows, top = route_ids.shape
    hit = [route_ids[:, k : k + 1] == jnp.arange(experts, dtype=jnp.int32)[None, :] for k in range(top)]
    named = sum(h.astype(jnp.float32) for h in hit)
    before = (jnp.arange(rows)[:, None] > jnp.arange(rows)[None, :]).astype(jnp.bfloat16)
    ranked = jnp.dot(before, named.astype(jnp.bfloat16), preferred_element_type=jnp.float32)
    base = ranked + jnp.arange(experts, dtype=jnp.float32)[None, :] * capacity
    return jnp.stack([jnp.sum(jnp.where(h, base, 0.0), axis=1) for h in hit])


def dispatch_matrix(places, first, count):
    slots = first + jnp.arange(count, dtype=jnp.int32)[:, None]
    hit = places[0][None, :] == slots
    for k in range(1, places.shape[0]):
        hit = hit | (places[k][None, :] == slots)
    return hit.astype(jnp.bfloat16)


def combine_matrix(places, weights, first, count):
    slots = first + jnp.arange(count, dtype=jnp.int32)[None, :]
    total = sum(
        jnp.where(places[k][:, None] == slots, weights[k][:, None], 0.0) for k in range(places.shape[0])
    )
    high = total.astype(jnp.bfloat16)
    low = (total - high.astype(jnp.float32)).astype(jnp.bfloat16)
    return high, low


def dot32(a, b):
    return jnp.dot(a, b, preferred_element_type=jnp.float32)


def hidden_of(rows, w_gate, w_up):
    gate_pre = dot32(rows, w_gate)
    up_pre = dot32(rows, w_up)
    return (jax.nn.silu(gate_pre) * up_pre).astype(jnp.bfloat16)


def body(tokens, norm_gain, route_ids, route_gates, w_gate, w_up, w_down):
    tok_rows, width = tokens.shape
    top_count = route_ids.shape[1]
    devices = lax.axis_size("ep")
    local_experts = w_gate.shape[0]
    experts = local_experts * devices
    capacity = 3 * tok_rows * top_count // (2 * experts)
    half = devices // 2
    me = lax.axis_index("ep")
    side = me // half
    groups = [list(range(half)), list(range(half, devices))]
    across = [(i, (i + half) % devices) for i in range(devices)]
    block = local_experts * capacity
    count = half * block
    first = side * count
    step = width // CHUNKS

    def cross(value):
        return lax.ppermute(value, "ep", across)

    def exchange(value):
        return lax.all_to_all(value, "ep", 0, 0, axis_index_groups=groups, tiled=True)

    normed = rms_norm(tokens, norm_gain)
    far = [cross(normed[:, c * step : (c + 1) * step]) for c in range(CHUNKS)]
    weights = (route_gates / jnp.sum(route_gates, axis=1, keepdims=True)).T
    places = slot_index(route_ids, experts, capacity)
    table = cross(jnp.concatenate([places, weights]))
    places, far_places = places.astype(jnp.int32), table[:top_count].astype(jnp.int32)
    far_weights = table[top_count:]

    def send(matrix, parts):
        got = [exchange(dot32(matrix, part).astype(jnp.bfloat16)) for part in parts]
        got = got[0] if len(got) == 1 else jnp.concatenate(got, axis=1)
        return got.reshape(half, local_experts, capacity, width)

    def finish(arrived):
        mids = []
        for j in range(local_experts):
            rows = arrived[:, j].reshape(half * capacity, width)
            mids.append(hidden_of(rows, w_gate[j], w_up[j]))

        def out(c):
            ends = [
                dot32(mids[j], w_down[j, :, c * step : (c + 1) * step])
                .astype(jnp.bfloat16)
                .reshape(half, 1, capacity, step)
                for j in range(local_experts)
            ]
            ends = ends[0] if local_experts == 1 else jnp.concatenate(ends, axis=1)
            return exchange(ends.reshape(count, step))

        return out

    own_out = finish(send(dispatch_matrix(places, first, count), [normed]))
    far_out = finish(send(dispatch_matrix(far_places, first, count), far))
    far_high, far_low = combine_matrix(far_places, far_weights, first, count)
    high, low = combine_matrix(places, weights, first, count)
    partial = []
    for c in range(CHUNKS):
        back = far_out(c)
        partial.append(cross((dot32(far_high, back) + dot32(far_low, back)).astype(jnp.bfloat16)))
    mixed = []
    for c in range(CHUNKS):
        back = own_out(c)
        total = dot32(high, back) + dot32(low, back) + partial[c].astype(jnp.float32)
        mixed.append(total.astype(jnp.bfloat16))
    return jnp.concatenate(mixed, axis=1)


def solution(mesh):
    placed = (
        P(("grp", "ep"), None),
        P(),
        P(("grp", "ep"), None),
        P(("grp", "ep"), None),
        P("ep", None, None),
        P("ep", None, None),
        P("ep", None, None),
    )
    return jax.shard_map(
        body, mesh=mesh, in_specs=placed, out_specs=P(("grp", "ep"), None), check_vma=False
    )
```

time: 382 us -> 360 us (0.942)
  blocking collectives: 144 us -> 0 us
  waiting for transfers between devices: 137 us -> 231 us
  matrix products: 23.2 us -> 67.1 us
  starting transfers between devices: 5.55 us -> 48.4 us
  local copies, waits for them, and re-layouts: 46.1 us -> 3.53 us
  other arithmetic: 25.1 us -> 5.05 us
    ppermute x0 -> x5, waiting for transfers between devices: none -> 156 us  [cross(): return lax.ppermute(value, 'ep', across)]
    all_to_all x1 -> x0, blocking collectives: 144 us -> none  [body(): lax.all_to_all(outgoing, 'ep', split_axis=0, concat_axis=0, tiled=True)]
    all_to_all x1 -> x7, waiting for transfers between devices: 137 us -> 75.3 us  [exchange(): lax.all_to_all(value, 'ep', 0, 0, axis_index_groups=groups, tiled=True)]
    dot_general x3 -> x20, matrix products: 23.2 us -> 67.1 us  [the longest x19 66.8 us: dot32(): return jnp.dot(a, b, preferred_element_type=jnp.float32)]
    all_to_all x1 -> x7, starting transfers between devices: 5.55 us -> 41.7 us  [exchange(): lax.all_to_all(value, 'ep', 0, 0, axis_index_groups=groups, tiled=True)]
    scatter x1 -> x0, local copies, waits for them, and re-layouts: 22 us -> none  [body(): jnp.zeros((experts * capacity, width), jnp.bfloat16).at[places]]
    reduce_sum x3 -> x1, other arithmetic: 15.1 us -> 0.02 us  [body(): weights = (route_gates / jnp.sum(route_gates, axis=1, keepdims=True)).T]
    gather x1 -> x0, local copies, waits for them, and re-layouts: 12.4 us -> none  [body(): picked = returned.reshape(experts * capacity, width)[places]]
  transfers between devices with their start and end apart: 1 -> 12, of which waited for: 1 -> 10; matrix products, arithmetic and copies ran while one was open for 0% -> 17% of each run, Pallas kernels for 0% -> 0%
where the time goes in v1:
time: 360 us; the launch traced here: 356 us
  waiting for transfers between devices  231 us (64%)
  matrix products  67.1 us (19%)
  starting transfers between devices  48.4 us (13%)
  other arithmetic  5.05 us (1%)
    ppermute x5, waiting for transfers between devices, cross(): return lax.ppermute(value, 'ep', across)  156 us
    all_to_all x7, waiting for transfers between devices, exchange(): lax.all_to_all(value, 'ep', 0, 0, axis_index_groups=groups, tiled=True)  75.3 us
    dot_general x19, matrix products, dot32(): return jnp.dot(a, b, preferred_element_type=jnp.float32)  66.8 us
    all_to_all x7, starting transfers between devices, exchange(): lax.all_to_all(value, 'ep', 0, 0, axis_index_groups=groups, tiled=True)  41.7 us
  transfers between devices with their start and end apart: 12, of which 10 were waited for; matrix products, arithmetic and copies ran while one was open for 17% of the time, Pallas kernels for 0%

profile of v1, /device:TPU:15, one launch (start us, length us, event | category | flops | bytes accessed | tf_op | source)
XLA Modules:
  0.0 355.5 jit_solution(18290334633392432660)
XLA Ops:
  7.5 45.3 %collective-permute-done = f32[4,512]{1,0:T(4,128)S(1)} collective-permute-done((f32[4,512]{1,0:T(4,128)S(1)}, f32[4,512]{1,0:T(4,128)S(1)}, u32[]{:S(2)}, u32[]{:S(2)}) %collective-permute-start) | collective-permute-done | bytes 8224 | tf_op jit(solution)/shard_map/ppermute | solution.py:72
  56.3 5.6 %all-to-all-start.2 = ((bf16[8,96,1024]{2,1,0:T(8,128)(2,1)}), bf16[8,96,1024]{2,1,0:T(8,128)(2,1)}, u32[]{:S(2)}, u32[]{:S(2)}) async-start(bf16[8,96,1024]{2,1,0:T(8,128)(2,1)} %bitcast.86), calls=%async_computation.2 | async-start | bytes 3145728 | tf_op jit(solution)/shard_map/all_to_all | solution.py:75
  63.8 44.6 %collective-permute-done.2 = bf16[512,1024]{1,0:T(8,128)(2,1)S(1)} collective-permute-done((bf16[512,1024]{1,0:T(8,128)(2,1)S(1)}, bf16[512,1024]{1,0:T(8,128)(2,1)S(1)}, u32[]{:S(2)}, u32[]{:S(2)}) %collective-permute-start.2) | collective-permute-done | bytes 1048608 | tf_op jit(solution)/shard_map/ppermute | solution.py:72
  110.6 6.6 %all-to-all-start.3 = ((bf16[8,96,1024]{2,1,0:T(8,128)(2,1)}), bf16[8,96,1024]{2,1,0:T(8,128)(2,1)}, u32[]{:S(2)}, u32[]{:S(2)}) async-start(bf16[8,96,1024]{2,1,0:T(8,128)(2,1)} %bitcast.85), calls=%async_computation.3 | async-start | bytes 3145728 | tf_op jit(solution)/shard_map/all_to_all | solution.py:75
  120.7 14.6 %all-to-all-done.3 = bf16[8,96,1024]{2,1,0:T(8,128)(2,1)} async-done(((bf16[8,96,1024]{2,1,0:T(8,128)(2,1)}), bf16[8,96,1024]{2,1,0:T(8,128)(2,1)}, u32[]{:S(2)}, u32[]{:S(2)}) %all-to-all-start.3) | async-done | bytes 1572896 | tf_op jit(solution)/shard_map/all_to_all | solution.py:75
  135.4 5.6 %all-to-all-start = ((bf16[8,96,2048]{2,1,0:T(8,128)(2,1)}), bf16[8,96,2048]{2,1,0:T(8,128)(2,1)S(1)}, u32[]{:S(2)}, u32[]{:S(2)}) async-start(bf16[8,96,2048]{2,1,0:T(8,128)(2,1)} %bitcast.79), calls=%async_computation | async-start | bytes 6291456 | tf_op jit(solution)/shard_map/all_to_all | solution.py:75
  141.0 6.4 %fusion.3 = f32[768,1024]{1,0:T(8,128)S(1)} fusion(bf16[1,2048,1024]{2,1,0:T(8,128)(2,1)} %param.12, bf16[768,1024]{1,0:T(8,128)(2,1)} %bitcast.23, bf16[768,1024]{1,0:T(8,128)(2,1)} %bitcast.21), kind=kOutput, calls=%fused_computation.5 | convolution fusion | flops 3227516928 | bytes 10485760 | tf_op jit(solution)/shard_map/dot_general | solution.py:45
  147.5 5.9 %multiply_convert_fusion = bf16[768,1024]{1,0:T(8,128)(2,1)S(1)} fusion(f32[768,1024]{1,0:T(8,128)S(1)} %fusion.3, bf16[1,2048,1024]{2,1,0:T(8,128)(2,1)S(1)} %copy-done.3, bf16[768,1024]{1,0:T(8,128)(2,1)} %bitcast.23, bf16[768,1024]{1,0:T(8,128)(2,1)} %bitcast.21), kind=kOutput, calls=%fused_computation.15 | convolution fusion | flops 3232235520 | bytes 12058624 | tf_op jit(solution)/shard_map/dot_general | solution.py:45
  157.5 18.4 %all-to-all-done = bf16[8,96,2048]{2,1,0:T(8,128)(2,1)S(1)} async-done(((bf16[8,96,2048]{2,1,0:T(8,128)(2,1)}), bf16[8,96,2048]{2,1,0:T(8,128)(2,1)S(1)}, u32[]{:S(2)}, u32[]{:S(2)}) %all-to-all-start) | async-done | bytes 3145760 | tf_op jit(solution)/shard_map/all_to_all | solution.py:75
  175.9 6.3 %all-to-all-start.4 = ((bf16[8,96,1024]{2,1,0:T(8,128)(2,1)}), bf16[8,96,1024]{2,1,0:T(8,128)(2,1)}, u32[]{:S(2)}, u32[]{:S(2)}) async-start(bf16[8,96,1024]{2,1,0:T(8,128)(2,1)} %bitcast.88), calls=%async_computation.4 | async-start | bytes 3145728 | tf_op jit(solution)/shard_map/all_to_all | solution.py:75
  182.2 5.0 %fusion.36 = bf16[768,1024]{1,0:T(8,128)(2,1)} fusion(bf16[768,1024]{1,0:T(8,128)(2,1)} %copy-done.8, bf16[1,1024,2048]{2,1,0:T(8,128)(2,1)} %param.13), kind=kOutput, calls=%fused_computation.39 | convolution fusion | flops 1611399168 | bytes 5242880 | tf_op jit(solution)/shard_map/dot_general | solution.py:45
  187.2 13.1 %all-to-all-done.4 = bf16[8,96,1024]{2,1,0:T(8,128)(2,1)} async-done(((bf16[8,96,1024]{2,1,0:T(8,128)(2,1)}), bf16[8,96,1024]{2,1,0:T(8,128)(2,1)}, u32[]{:S(2)}, u32[]{:S(2)}) %all-to-all-start.4) | async-done | bytes 1572896 | tf_op jit(solution)/shard_map/all_to_all | solution.py:75
  200.3 6.3 %all-to-all-start.6 = ((bf16[8,96,1024]{2,1,0:T(8,128)(2,1)}), bf16[8,96,1024]{2,1,0:T(8,128)(2,1)}, u32[]{:S(2)}, u32[]{:S(2)}) async-start(bf16[8,96,1024]{2,1,0:T(8,128)(2,1)} %bitcast.87), calls=%async_computation.6 | async-start | bytes 3145728 | tf_op jit(solution)/shard_map/all_to_all | solution.py:75
  206.6 5.3 %fusion.5 = f32[768,1024]{1,0:T(8,128)S(1)} fusion(bf16[768,2048]{1,0:T(8,128)(2,1)S(1)} %bitcast.77, bf16[1,2048,1024]{2,1,0:T(8,128)(2,1)} %param.12), kind=kOutput, calls=%fused_computation.7 | convolution fusion | flops 3221225472 | bytes 10485760 | tf_op jit(solution)/shard_map/dot_general | solution.py:45
  211.9 3.8 %multiply_convert_fusion.1 = bf16[768,1024]{1,0:T(8,128)(2,1)S(1)} fusion(f32[768,1024]{1,0:T(8,128)S(1)} %fusion.5, bf16[768,2048]{1,0:T(8,128)(2,1)S(1)} %bitcast.78, bf16[1,2048,1024]{2,1,0:T(8,128)(2,1)S(1)} %copy-done.4), kind=kOutput, calls=%fused_computation.16 | convolution fusion | flops 3225944064 | bytes 12058624 | tf_op jit(solution)/shard_map/dot_general | solution.py:45
  219.8 4.8 %all-to-all-done.6 = bf16[8,96,1024]{2,1,0:T(8,128)(2,1)} async-done(((bf16[8,96,1024]{2,1,0:T(8,128)(2,1)}), bf16[8,96,1024]{2,1,0:T(8,128)(2,1)}, u32[]{:S(2)}, u32[]{:S(2)}) %all-to-all-start.6) | async-done | bytes 1572896 | tf_op jit(solution)/shard_map/all_to_all | solution.py:75
  224.7 5.7 %all-to-all-start.1 = ((bf16[8,96,1024]{2,1,0:T(8,128)(2,1)}), bf16[8,96,1024]{2,1,0:T(8,128)(2,1)S(1)}, u32[]{:S(2)}, u32[]{:S(2)}) async-start(bf16[8,96,1024]{2,1,0:T(8,128)(2,1)} %bitcast.14), calls=%async_computation.1 | async-start | bytes 3145728 | tf_op jit(solution)/shard_map/all_to_all | solution.py:75
  230.4 4.5 %fusion.33 = bf16[768,1024]{1,0:T(8,128)(2,1)} fusion(bf16[768,1024]{1,0:T(8,128)(2,1)S(1)} %copy-done.10, bf16[1,1024,2048]{2,1,0:T(8,128)(2,1)} %param.13), kind=kOutput, calls=%fused_computation.38 | convolution fusion | flops 1611399168 | bytes 5242880 | tf_op jit(solution)/shard_map/dot_general | solution.py:45
  234.9 13.5 %all-to-all-done.1 = bf16[8,96,1024]{2,1,0:T(8,128)(2,1)S(1)} async-done(((bf16[8,96,1024]{2,1,0:T(8,128)(2,1)}), bf16[8,96,1024]{2,1,0:T(8,128)(2,1)S(1)}, u32[]{:S(2)}, u32[]{:S(2)}) %all-to-all-start.1) | async-done | bytes 1572896 | tf_op jit(solution)/shard_map/all_to_all | solution.py:75
  248.4 5.6 %all-to-all-start.5 = ((bf16[8,96,1024]{2,1,0:T(8,128)(2,1)}), bf16[8,96,1024]{2,1,0:T(8,128)(2,1)S(1)}, u32[]{:S(2)}, u32[]{:S(2)}) async-start(bf16[8,96,1024]{2,1,0:T(8,128)(2,1)} %bitcast.84), calls=%async_computation.5 | async-start | bytes 3145728 | tf_op jit(solution)/shard_map/all_to_all | solution.py:75
  264.3 3.6 %add_convert_fusion.1 = bf16[512,1024]{1,0:T(8,128)(2,1)} fusion(f32[512,1024]{1,0:T(8,128)S(1)} %fusion.57, bf16[768,1024]{1,0:T(8,128)(2,1)} %bitcast.30, f32[512]{0:T(512)S(1)} %bitcast.130, f32[512]{0:T(512)S(1)} %bitcast.126, s32[768]{0:T(1024)S(1)} %iota_add_fusion, s32[512]{0:T(512)S(1)} %bitcast.104, s32[512]{0:T(512)S(1)} %bitcast.98), kind=kOutput, calls=%fused_computation.27 | convolution fusion | flops 809893888 | bytes 4729856 | tf_op jit(solution)/shard_map/dot_general | solution.py:45
  271.2 10.9 %all-to-all-done.5 = bf16[8,96,1024]{2,1,0:T(8,128)(2,1)S(1)} async-done(((bf16[8,96,1024]{2,1,0:T(8,128)(2,1)}), bf16[8,96,1024]{2,1,0:T(8,128)(2,1)S(1)}, u32[]{:S(2)}, u32[]{:S(2)}) %all-to-all-start.5) | async-done | bytes 1572896 | tf_op jit(solution)/shard_map/all_to_all | solution.py:75
  283.2 45.9 %collective-permute-done.3 = bf16[512,1024]{1,0:T(8,128)(2,1)} collective-permute-done((bf16[512,1024]{1,0:T(8,128)(2,1)}, bf16[512,1024]{1,0:T(8,128)(2,1)}, u32[]{:S(2)}, u32[]{:S(2)}) %collective-permute-start.3) | collective-permute-done | bytes 1048608 | tf_op jit(solution)/shard_map/ppermute | solution.py:72
  331.6 20.0 %collective-permute-done.4 = bf16[512,1024]{1,0:T(8,128)(2,1)} collective-permute-done((bf16[512,1024]{1,0:T(8,128)(2,1)}, bf16[512,1024]{1,0:T(8,128)(2,1)}, u32[]{:S(2)}, u32[]{:S(2)}) %collective-permute-start.4) | collective-permute-done | bytes 1048608 | tf_op jit(solution)/shard_map/ppermute | solution.py:72
  (59 shorter events, 47.8 us)
Async XLA Ops:
  0.0 2.2 copy-start
  3.5 3.5 copy-start.2
  3.5 3.5 copy-start.1
  4.7 48.1 %collective-permute-start.1 = (bf16[512,1024]{1,0:T(8,128)(2,1)}, bf16[512,1024]{1,0:T(8,128)(2,1)}, u32[]{:S(2)}, u32[]{:S(2)}) collective-permute-start(bf16[512,1024]{1,0:T(8,128)(2,1)} %get-tuple-element.7), channel_id=1, source_target_pairs={{0,8},{1,9},{2,10},{3,11},{4,12},{5,13},{6,14},{7,15},{8,0},{9,1},... | collective-permute-start | bytes 3145736 | tf_op jit(solution)/shard_map/ppermute | solution.py:72
  7.4 45.5 %collective-permute-start = (f32[4,512]{1,0:T(4,128)S(1)}, f32[4,512]{1,0:T(4,128)S(1)}, u32[]{:S(2)}, u32[]{:S(2)}) collective-permute-start(f32[4,512]{1,0:T(4,128)S(1)} %pad_maximum_fusion.4), channel_id=1, source_target_pairs={{0,8},{1,9},{2,10},{3,11},{4,12},{5,13},{6,14},{7,15},{8,0},{9,1},... | collective-permute-start | bytes 24584 | tf_op jit(solution)/shard_map/ppermute | solution.py:72
  56.3 54.3 %all-to-all-start.2 = ((bf16[8,96,1024]{2,1,0:T(8,128)(2,1)}), bf16[8,96,1024]{2,1,0:T(8,128)(2,1)}, u32[]{:S(2)}, u32[]{:S(2)}) async-start(bf16[8,96,1024]{2,1,0:T(8,128)(2,1)} %bitcast.86), calls=%async_computation.2 | async-start | bytes 3145728 | tf_op jit(solution)/shard_map/all_to_all | solution.py:75
  61.9 46.5 %collective-permute-start.2 = (bf16[512,1024]{1,0:T(8,128)(2,1)S(1)}, bf16[512,1024]{1,0:T(8,128)(2,1)S(1)}, u32[]{:S(2)}, u32[]{:S(2)}) collective-permute-start(bf16[512,1024]{1,0:T(8,128)(2,1)S(1)} %get-tuple-element.8), channel_id=1, source_target_pairs={{0,8},{1,9},{2,10},{3,11},{4,12},{5,13},{6,14},{7,15},{8,0},{9,1},... | collective-permute-start | bytes 3145736 | tf_op jit(solution)/shard_map/ppermute | solution.py:72
  110.6 24.8 %all-to-all-start.3 = ((bf16[8,96,1024]{2,1,0:T(8,128)(2,1)}), bf16[8,96,1024]{2,1,0:T(8,128)(2,1)}, u32[]{:S(2)}, u32[]{:S(2)}) async-start(bf16[8,96,1024]{2,1,0:T(8,128)(2,1)} %bitcast.85), calls=%async_computation.3 | async-start | bytes 3145728 | tf_op jit(solution)/shard_map/all_to_all | solution.py:75
  135.4 40.5 %all-to-all-start = ((bf16[8,96,2048]{2,1,0:T(8,128)(2,1)}), bf16[8,96,2048]{2,1,0:T(8,128)(2,1)S(1)}, u32[]{:S(2)}, u32[]{:S(2)}) async-start(bf16[8,96,2048]{2,1,0:T(8,128)(2,1)} %bitcast.79), calls=%async_computation | async-start | bytes 6291456 | tf_op jit(solution)/shard_map/all_to_all | solution.py:75
  141.0 6.4 %copy-start.3 = (bf16[1,2048,1024]{2,1,0:T(8,128)(2,1)S(1)}, bf16[1,2048,1024]{2,1,0:T(8,128)(2,1)}, u32[]{:S(2)}) copy-start(bf16[1,2048,1024]{2,1,0:T(8,128)(2,1)} %param.11) | copy-start | bytes 12582916
  147.5 7.1 %copy-start.5 = (bf16[1,1024,2048]{2,1,0:T(8,128)(2,1)S(1)}, bf16[1,1024,2048]{2,1,0:T(8,128)(2,1)}, u32[]{:S(2)}) copy-start(bf16[1,1024,2048]{2,1,0:T(8,128)(2,1)} %param.13) | copy-start | bytes 12582916
  153.4 1.1 copy-start.8
  175.9 24.4 %all-to-all-start.4 = ((bf16[8,96,1024]{2,1,0:T(8,128)(2,1)}), bf16[8,96,1024]{2,1,0:T(8,128)(2,1)}, u32[]{:S(2)}, u32[]{:S(2)}) async-start(bf16[8,96,1024]{2,1,0:T(8,128)(2,1)} %bitcast.88), calls=%async_computation.4 | async-start | bytes 3145728 | tf_op jit(solution)/shard_map/all_to_all | solution.py:75
  200.3 24.4 %all-to-all-start.6 = ((bf16[8,96,1024]{2,1,0:T(8,128)(2,1)}), bf16[8,96,1024]{2,1,0:T(8,128)(2,1)}, u32[]{:S(2)}, u32[]{:S(2)}) async-start(bf16[8,96,1024]{2,1,0:T(8,128)(2,1)} %bitcast.87), calls=%async_computation.6 | async-start | bytes 3145728 | tf_op jit(solution)/shard_map/all_to_all | solution.py:75
  206.6 5.4 %copy-start.4 = (bf16[1,2048,1024]{2,1,0:T(8,128)(2,1)S(1)}, bf16[1,2048,1024]{2,1,0:T(8,128)(2,1)}, u32[]{:S(2)}) copy-start(bf16[1,2048,1024]{2,1,0:T(8,128)(2,1)} %param.11) | copy-start | bytes 12582916
  211.9 4.9 %copy-start.6 = (bf16[1,1024,2048]{2,1,0:T(8,128)(2,1)S(1)}, bf16[1,1024,2048]{2,1,0:T(8,128)(2,1)}, u32[]{:S(2)}) copy-start(bf16[1,1024,2048]{2,1,0:T(8,128)(2,1)} %param.13) | copy-start | bytes 12582916
  215.7 1.1 copy-start.9
  224.7 5.7 %copy-start.10 = (bf16[768,1024]{1,0:T(8,128)(2,1)S(1)}, bf16[768,1024]{1,0:T(8,128)(2,1)}, u32[]{:S(2)}) copy-start(bf16[768,1024]{1,0:T(8,128)(2,1)} %copy-done.9) | copy-start | bytes 4718596
  224.7 23.7 %all-to-all-start.1 = ((bf16[8,96,1024]{2,1,0:T(8,128)(2,1)}), bf16[8,96,1024]{2,1,0:T(8,128)(2,1)S(1)}, u32[]{:S(2)}, u32[]{:S(2)}) async-start(bf16[8,96,1024]{2,1,0:T(8,128)(2,1)} %bitcast.14), calls=%async_computation.1 | async-start | bytes 3145728 | tf_op jit(solution)/shard_map/all_to_all | solution.py:75
  248.4 33.6 %all-to-all-start.5 = ((bf16[8,96,1024]{2,1,0:T(8,128)(2,1)}), bf16[8,96,1024]{2,1,0:T(8,128)(2,1)S(1)}, u32[]{:S(2)}, u32[]{:S(2)}) async-start(bf16[8,96,1024]{2,1,0:T(8,128)(2,1)} %bitcast.84), calls=%async_computation.5 | async-start | bytes 3145728 | tf_op jit(solution)/shard_map/all_to_all | solution.py:75
  260.2 69.0 %collective-permute-start.3 = (bf16[512,1024]{1,0:T(8,128)(2,1)}, bf16[512,1024]{1,0:T(8,128)(2,1)}, u32[]{:S(2)}, u32[]{:S(2)}) collective-permute-start(bf16[512,1024]{1,0:T(8,128)(2,1)} %add_convert_fusion.3), channel_id=1, source_target_pairs={{0,8},{1,9},{2,10},{3,11},{4,12},{5,13},{6,14},{7,15},{8,0},{9,1},... | collective-permute-start | bytes 3145736 | tf_op jit(solution)/shard_map/ppermute | solution.py:72
  267.8 83.7 %collective-permute-start.4 = (bf16[512,1024]{1,0:T(8,128)(2,1)}, bf16[512,1024]{1,0:T(8,128)(2,1)}, u32[]{:S(2)}, u32[]{:S(2)}) collective-permute-start(bf16[512,1024]{1,0:T(8,128)(2,1)} %add_convert_fusion.1), channel_id=1, source_target_pairs={{0,8},{1,9},{2,10},{3,11},{4,12},{5,13},{6,14},{7,15},{8,0},{9,1},... | collective-permute-start | bytes 3145736 | tf_op jit(solution)/shard_map/ppermute | solution.py:72
  282.0 47.1 %copy-start.7 = (f32[512,1024]{1,0:T(8,128)S(1)}, f32[512,1024]{1,0:T(8,128)}, u32[]{:S(2)}) copy-start(f32[512,1024]{1,0:T(8,128)} %fusion.55) | copy-start | bytes 6291460

commit v2 on v0

v2 whole, which is shorter than its diff:
```python
import functools

import jax
import jax.numpy as jnp
from jax import lax
from jax.experimental import pallas as pl
from jax.experimental.pallas import tpu as pltpu
from jax.sharding import PartitionSpec as P

EPS = 1e-06
CHUNKS = 4
TILE = 256
VMEM_BYTES = 66000000


def rms_norm(tokens, norm_gain):
    floats = tokens.astype(jnp.float32)
    scale = lax.rsqrt(jnp.mean(floats * floats, axis=-1, keepdims=True) + EPS)
    return (floats * scale * norm_gain).astype(jnp.bfloat16)


def slot_index(route_ids, experts, capacity):
    rows, top = route_ids.shape
    hit = [route_ids[:, k : k + 1] == jnp.arange(experts, dtype=jnp.int32)[None, :] for k in range(top)]
    named = sum(h.astype(jnp.float32) for h in hit)
    before = (jnp.arange(rows)[:, None] > jnp.arange(rows)[None, :]).astype(jnp.bfloat16)
    ranked = jnp.dot(before, named.astype(jnp.bfloat16), preferred_element_type=jnp.float32)
    base = ranked + jnp.arange(experts, dtype=jnp.float32)[None, :] * capacity
    return jnp.stack([jnp.sum(jnp.where(h, base, 0.0), axis=1) for h in hit])


def dot32(a, b):
    return jnp.dot(a, b, preferred_element_type=jnp.float32)


def kernel(
    devices, capacity, top,
    normed, table, gate_hbm, up_hbm, down_hbm,
    mixed,
    far, far_table, takes, highs, lows, packed, arrived, hidden, w_gate, w_up, w_down,
    outs, backs, partial, partial_in,
    weight_sems, table_sems, far_send, far_recv, own_sems, self_sems, go_send, go_recv,
    back_send, back_recv, part_send, part_recv,
):
    half = devices // 2
    chunks, rows, step = normed.shape
    count = half * capacity
    ff = w_gate.shape[1]
    me = lax.axis_index("ep")
    q = me % half
    base = me - q
    partner = (me + half) % devices
    first = base * capacity

    def peer_at(i):
        off = (half // 2 + i) % half + (half // 2 + i) // half
        return (q + off) % half

    barrier = pltpu.get_barrier_semaphore()

    def greet(i, carry):
        pl.semaphore_signal(barrier, inc=1, device_id={"ep": base + peer_at(i)})
        return carry

    lax.fori_loop(0, half - 1, greet, 0)
    pl.semaphore_signal(barrier, inc=1, device_id={"ep": partner})

    loads = [
        pltpu.make_async_copy(gate_hbm.at[0], w_gate, weight_sems.at[0]),
        pltpu.make_async_copy(up_hbm.at[0], w_up, weight_sems.at[1]),
        pltpu.make_async_copy(down_hbm.at[0], w_down, weight_sems.at[2]),
    ]
    pl.semaphore_wait(barrier, half)

    def remote(src, dst, send, recv, device):
        return pltpu.make_async_remote_copy(
            src_ref=src, dst_ref=dst, send_sem=send, recv_sem=recv, device_id={"ep": device}
        )

    def table_copy():
        return remote(table, far_table, table_sems.at[0], table_sems.at[1], partner)

    def far_copy(c):
        return remote(normed.at[c], far.at[c], far_send.at[c], far_recv.at[c], partner)

    def part_copy(c):
        return remote(partial.at[c], partial_in.at[c], part_send.at[c], part_recv.at[c], partner)

    def span(j):
        return pl.ds(pl.multiple_of(j * capacity, 16), capacity)

    def go_copy(s, c, peer, slot):
        return remote(
            packed.at[s, c, span(peer)], arrived.at[s, c, span(q)],
            go_send.at[s, c, slot], go_recv.at[s, c, q], base + peer,
        )

    def back_copy(s, c, peer, slot):
        return remote(
            outs.at[s, c, span(peer)], backs.at[s, c, span(q)],
            back_send.at[s, c, slot], back_recv.at[s, c, q], base + peer,
        )

    def go_arrival(s, c, peer):
        return remote(
            packed.at[s, c, span(peer)], arrived.at[s, c, span(peer)],
            go_send.at[s, c, 0], go_recv.at[s, c, peer], base + peer,
        )

    def back_arrival(s, c, peer):
        return remote(
            outs.at[s, c, span(peer)], backs.at[s, c, span(peer)],
            back_send.at[s, c, 0], back_recv.at[s, c, peer], base + peer,
        )

    def go_self(s, c):
        return pltpu.make_async_copy(packed.at[s, c, span(q)], arrived.at[s, c, span(q)], own_sems.at[s, c])

    def back_self(s, c):
        return pltpu.make_async_copy(outs.at[s, c, span(q)], backs.at[s, c, span(q)], self_sems.at[s, c])

    def each_peer(act):
        def one(i, carry):
            act(peer_at(i), i)
            return carry

        lax.fori_loop(0, half - 1, one, 0)

    def matrices(s, source):
        width = 128

        def one(i, carry):
            at = pl.multiple_of(i * width, width)
            slots = (first + at + lax.broadcasted_iota(jnp.int32, (width, rows), 0)).astype(jnp.float32)
            taken = jnp.zeros((width, rows), jnp.float32)
            total = jnp.zeros((width, rows), jnp.float32)
            for k in range(top):
                hit = source[k : k + 1, :] == slots
                taken = taken + jnp.where(hit, 1.0, 0.0)
                total = total + jnp.where(hit, source[top + k : top + k + 1, :], 0.0)
            takes[s, pl.ds(at, width), :] = taken.astype(jnp.bfloat16)
            turned = total.T
            high = turned.astype(jnp.bfloat16)
            highs[s, :, pl.ds(at, width)] = high
            lows[s, :, pl.ds(at, width)] = (turned - high.astype(jnp.float32)).astype(jnp.bfloat16)
            return carry

        lax.fori_loop(0, count // width, one, 0)

    def tiles(act):
        def one(i, carry):
            act(pl.ds(pl.multiple_of(i * TILE, TILE), TILE))
            return carry

        lax.fori_loop(0, step // TILE, one, 0)

    def pack(s, c, source):
        def one(cols):
            packed[s, c, :, cols] = dot32(takes[s], source[c, :, cols]).astype(jnp.bfloat16)

        tiles(one)
        each_peer(lambda peer, i: go_copy(s, c, peer, i).start())
        go_self(s, c).start()

    def wait_go(s, c):
        each_peer(lambda peer, i: go_arrival(s, c, peer).wait_recv())
        go_self(s, c).wait()

    def expert_hidden(s):
        def one(i, carry):
            cols = pl.ds(pl.multiple_of(i * TILE, TILE), TILE)
            gate_pre = dot32(arrived[s, 0], w_gate[0:step, cols])
            up_pre = dot32(arrived[s, 0], w_up[0:step, cols])
            for c in range(1, chunks):
                gate_pre += dot32(arrived[s, c], w_gate[c * step : (c + 1) * step, cols])
                up_pre += dot32(arrived[s, c], w_up[c * step : (c + 1) * step, cols])
            hidden[s, :, cols] = (gate_pre / (1.0 + jnp.exp(-gate_pre)) * up_pre).astype(jnp.bfloat16)
            return carry

        lax.fori_loop(0, ff // TILE, one, 0)

    def expert_out(s, c):
        def one(i, carry):
            at = pl.multiple_of(i * TILE, TILE)
            cols = pl.ds(pl.multiple_of(c * step + at, TILE), TILE)
            outs[s, c, :, pl.ds(at, TILE)] = dot32(hidden[s], w_down[:, cols]).astype(jnp.bfloat16)
            return carry

        lax.fori_loop(0, step // TILE, one, 0)

    def send_back(s, c):
        each_peer(lambda peer, i: back_copy(s, c, peer, i).start())
        back_self(s, c).start()

    def wait_back(s, c):
        each_peer(lambda peer, i: back_arrival(s, c, peer).wait_recv())
        back_self(s, c).wait()

    table_copy().start()
    far_copy(0).start()
    for load in loads:
        load.start()
    matrices(0, table)
    for c in range(chunks):
        pack(0, c, normed)
        if c + 1 < chunks:
            far_copy(c + 1).start()
    table_copy().wait()
    matrices(1, far_table)
    for c in range(chunks):
        far_copy(c).wait_recv()
        pack(1, c, far)
        if c == chunks - 2:
            for s_c in range(chunks):
                wait_go(0, s_c)
            for load in loads:
                load.wait()
            expert_hidden(0)
            for d in range(chunks):
                expert_out(0, d)
    for c in range(chunks):
        wait_go(1, c)
    expert_hidden(1)
    for c in range(chunks):
        expert_out(1, c)
        send_back(1, c)
    for c in range(chunks):
        wait_back(1, c)

        def merge(cols):
            back = backs[1, c, :, cols]
            partial[c, :, cols] = (dot32(highs[1], back) + dot32(lows[1], back)).astype(jnp.bfloat16)

        tiles(merge)
        part_copy(c).start()
        send_back(0, c)
    for c in range(chunks):
        wait_back(0, c)
        part_copy(c).wait_recv()

        def close(i, carry):
            at = pl.multiple_of(i * TILE, TILE)
            cols = pl.ds(at, TILE)
            back = backs[0, c, :, cols]
            total = dot32(highs[0], back) + dot32(lows[0], back) + partial_in[c, :, cols].astype(jnp.float32)
            mixed[:, pl.ds(pl.multiple_of(c * step + at, TILE), TILE)] = total.astype(jnp.bfloat16)
            return carry

        lax.fori_loop(0, step // TILE, close, 0)
    for c in range(chunks):
        far_copy(c).wait_send()
        part_copy(c).wait_send()
        for s in range(2):
            each_peer(lambda peer, i: go_copy(s, c, peer, i).wait_send())
            each_peer(lambda peer, i: back_copy(s, c, peer, i).wait_send())


def body(tokens, norm_gain, route_ids, route_gates, w_gate, w_up, w_down):
    rows, width = tokens.shape
    top = route_ids.shape[1]
    devices = lax.axis_size("ep")
    experts = devices
    ff = w_gate.shape[2]
    capacity = 3 * rows * top // (2 * experts)
    half = devices // 2
    count = half * capacity
    step = width // CHUNKS
    normed = rms_norm(tokens, norm_gain).reshape(rows, CHUNKS, step).transpose(1, 0, 2)
    weights = (route_gates / jnp.sum(route_gates, axis=1, keepdims=True)).T
    table = jnp.concatenate([slot_index(route_ids, experts, capacity), weights])
    vmem = pl.BlockSpec(memory_space=pltpu.VMEM)
    hbm = pl.BlockSpec(memory_space=pl.ANY)
    bf16 = jnp.bfloat16
    dma = pltpu.SemaphoreType.DMA
    return pl.pallas_call(
        functools.partial(kernel, devices, capacity, top),
        out_shape=jax.ShapeDtypeStruct((rows, width), bf16),
        in_specs=[vmem, vmem, hbm, hbm, hbm],
        out_specs=vmem,
        scratch_shapes=[
            pltpu.VMEM((CHUNKS, rows, step), bf16),
            pltpu.VMEM(table.shape, jnp.float32),
            pltpu.VMEM((2, count, rows), bf16),
            pltpu.VMEM((2, rows, count), bf16),
            pltpu.VMEM((2, rows, count), bf16),
            pltpu.VMEM((2, CHUNKS, count, step), bf16),
            pltpu.VMEM((2, CHUNKS, count, step), bf16),
            pltpu.VMEM((2, count, ff), bf16),
            pltpu.VMEM((width, ff), bf16),
            pltpu.VMEM((width, ff), bf16),
            pltpu.VMEM((ff, width), bf16),
            pltpu.VMEM((2, CHUNKS, count, step), bf16),
            pltpu.VMEM((2, CHUNKS, count, step), bf16),
            pltpu.VMEM((CHUNKS, rows, step), bf16),
            pltpu.VMEM((CHUNKS, rows, step), bf16),
            dma((3,)),
            dma((2,)),
            dma((CHUNKS,)),
            dma((CHUNKS,)),
            dma((2, CHUNKS)),
            dma((2, CHUNKS)),
            dma((2, CHUNKS, half)),
            dma((2, CHUNKS, half)),
            dma((2, CHUNKS, half)),
            dma((2, CHUNKS, half)),
            dma((CHUNKS,)),
            dma((CHUNKS,)),
        ],
        compiler_params=pltpu.CompilerParams(
            collective_id=0, has_side_effects=True, vmem_limit_bytes=VMEM_BYTES
        ),
    )(normed, table, w_gate, w_up, w_down)


def solution(mesh):
    placed = (
        P(("grp", "ep"), None),
        P(),
        P(("grp", "ep"), None),
        P(("grp", "ep"), None),
        P("ep", None, None),
        P("ep", None, None),
        P("ep", None, None),
    )
    return jax.shard_map(
        body, mesh=mesh, in_specs=placed, out_specs=P(("grp", "ep"), None), check_vma=False
    )
```

time: 382 us -> 265 us (0.69)
  Pallas kernels: 0 us -> 249 us
  blocking collectives: 144 us -> 0 us
  waiting for transfers between devices: 137 us -> 0 us
  local copies, waits for them, and re-layouts: 46.1 us -> 10.9 us
  matrix products: 23.2 us -> 0.26 us
  other arithmetic: 25.1 us -> 4.4 us
  starting transfers between devices: 5.55 us -> 0 us
    pallas_call x0 -> x1, Pallas kernels: none -> 249 us  [body(): pl.pallas_call(functools.partial(kernel, devices, capacity, top), out_sha...]
    all_to_all x1 -> x0, blocking collectives: 144 us -> none  [body(): lax.all_to_all(outgoing, 'ep', split_axis=0, concat_axis=0, tiled=True)]
    all_to_all x1 -> x0, waiting for transfers between devices: 137 us -> none  [body(): lax.all_to_all(finished, 'ep', split_axis=0, concat_axis=0, tiled=True)]
    dot_general x3 -> x1, matrix products: 23.2 us -> 0.26 us  [slot_index(): jnp.dot(before, named.astype(jnp.bfloat16), preferred_element_type=jnp.fl...]
    scatter x1 -> x0, local copies, waits for them, and re-layouts: 22 us -> none  [body(): jnp.zeros((experts * capacity, width), jnp.bfloat16).at[places]]
    reduce_sum x3 -> x1, other arithmetic: 15.1 us -> 0.71 us  [body(): weights = (route_gates / jnp.sum(route_gates, axis=1, keepdims=True)).T]
    gather x1 -> x0, local copies, waits for them, and re-layouts: 12.4 us -> none  [body(): picked = returned.reshape(experts * capacity, width)[places]]
    convert_element_type x1 -> x0, local copies, waits for them, and re-layouts: 9.65 us -> none  [body(): shaped = picked.astype(jnp.float32).reshape(tok_rows, top_count, width)]
  transfers between devices with their start and end apart: 1 -> 0, of which waited for: 1 -> 0; matrix products, arithmetic and copies ran while one was open for 0% -> 0% of each run, Pallas kernels for 0% -> 0%
where the time goes in v2:
time: 265 us; the launch traced here: 264 us
  Pallas kernels  249 us (94%)
  local copies, waits for them, and re-layouts  10.9 us (4%)
  other arithmetic  4.4 us (2%)
    pallas_call x1, Pallas kernels, body(): pl.pallas_call(functools.partial(kernel, devices, capacity, top), out_sha...  249 us
    unnamed x4, local copies, waits for them, and re-layouts  6.02 us

profile of v2, /device:TPU:15, one launch (start us, length us, event | category | flops | bytes accessed | tf_op | source)
XLA Modules:
  0.0 264.5 jit_solution(656897400950655770)
XLA Ops:
  0.0 0.0 copy-start
  0.0 0.7 reduce_sum.39
  0.7 0.7 divide_bitcast_fusion
  1.4 0.8 fusion.5
  2.2 0.3 select_reduce_fusion.1
  2.4 0.6 pad_maximum_fusion.table
  3.1 2.9 %copy.8 = bf16[512,2048]{0,1:T(8,128)(2,1)S(1)} copy(bf16[512,2048]{1,0:T(8,128)(2,1)} %param.7) | data formatting | bytes 4194304 | tf_op args[0]
  5.9 0.5 fusion
  6.4 0.0 copy-done
  6.4 1.9 fusion.2
  8.3 4.1 %copy.9 = bf16[512,4,512]{2,0,1:T(8,128)(2,1)} copy(bf16[512,4,512]{0,2,1:T(8,128)(2,1)} %bitcast.8) | data formatting | bytes 4194304 | tf_op jit(solution)/shard_map/reshape | solution.py:268
  12.5 248.9 %shard_map.73 = bf16[512,2048]{1,0:T(8,128)(2,1)} custom-call(bf16[4,512,512]{2,1,0:T(8,128)(2,1)} %bitcast.9, f32[4,512]{1,0:T(4,128)} %pad_maximum_fusion.table, bf16[1,2048,1024]{2,1,0:T(8,128)(2,1)} %gate_hbm.1, bf16[1,2048,1024]{2,1,0:T(8,128)(2,1)} %up_hbm.1, bf16[1,1024,2048]{2,1,0:T(8,128)(2,1)} %down_hbm.1), custom_call_target="tpu_custom_call" | custom-call | tf_op jit(solution)/shard_map/pallas_call | solution.py:275
  261.3 3.2 %copy.11 = bf16[512,2048]{1,0:T(8,128)(2,1)} copy(bf16[512,2048]{1,0:T(8,128)(2,1)} %shard_map.73) | data formatting | bytes 4194304
  (2 shorter events, 0.0 us)
Async XLA Ops:
  0.0 6.4 %copy-start = (f32[2048]{0:T(1024)S(1)}, f32[2048]{0:T(1024)}, u32[]{:S(2)}) copy-start(f32[2048]{0:T(1024)} %param.8) | copy-start | bytes 24580

commit v3 on v0

v3 whole, which is shorter than its diff:
```python
import functools

import jax
import jax.numpy as jnp
from jax import lax
from jax.experimental import pallas as pl
from jax.experimental.pallas import tpu as pltpu
from jax.sharding import PartitionSpec as P

EPS = 1e-06
CHUNKS = 4
TILE = 256
VMEM_BYTES = 67000000


def slot_index(route_ids, experts, capacity):
    rows, top = route_ids.shape
    hit = [route_ids[:, k : k + 1] == jnp.arange(experts, dtype=jnp.int32)[None, :] for k in range(top)]
    named = sum(h.astype(jnp.float32) for h in hit)
    before = (jnp.arange(rows)[:, None] > jnp.arange(rows)[None, :]).astype(jnp.bfloat16)
    ranked = jnp.dot(before, named.astype(jnp.bfloat16), preferred_element_type=jnp.float32)
    base = ranked + jnp.arange(experts, dtype=jnp.float32)[None, :] * capacity
    return jnp.stack([jnp.sum(jnp.where(h, base, 0.0), axis=1) for h in hit])


def dot32(a, b):
    return jnp.dot(a, b, preferred_element_type=jnp.float32)


def kernel(
    devices, capacity, top,
    tokens_hbm, gain, table, gate_hbm, up_hbm, down_hbm,
    mixed,
    normed, near, far_in, far_out, tables, takes, highs, packed, packed_o, arrived, hidden,
    w_gate, w_up, w_down, backs, backs_o, sum_own, sum_near,
    load_sems, table_send, table_recv, near_send, near_recv, fin_send, fin_recv, fout_send, fout_recv,
    go_send, go_recv, goo_send, back_send, back_recv, backo_recv, self_go, self_back,
    own_send, own_recv, rel_send, rel_recv, up_send, up_recv,
):
    half, quarter = devices // 2, devices // 4
    chunks, rows, step = normed.shape
    count = half * capacity
    ff = w_gate.shape[1]
    width = chunks * step
    me = lax.axis_index("ep")
    place, p = me // quarter, me % quarter
    side = me // half
    q = me % half
    base = side * half
    plane = place * quarter
    inner_plane = (1 + side) * quarter
    inner_dev = inner_plane + p
    outer_dev = 3 * side * quarter + p
    far_dev = (2 - side) * quarter + p
    is_inner = place == 1 + side
    is_outer = place != 1 + side
    outer_plane_q = (1 - (place - 2 * side)) * quarter

    def peer_at(i):
        off = (half // 2 + i) % half + (half // 2 + i) // half
        return (q + off) % half

    barrier = pltpu.get_barrier_semaphore()

    def greet(i, carry):
        pl.semaphore_signal(barrier, inc=1, device_id={"ep": base + peer_at(i)})
        return carry

    loads = [
        pltpu.make_async_copy(gate_hbm.at[0], w_gate, load_sems.at[0]),
        pltpu.make_async_copy(up_hbm.at[0], w_up, load_sems.at[1]),
        pltpu.make_async_copy(down_hbm.at[0], w_down, load_sems.at[2]),
    ]
    token_load = pltpu.make_async_copy(tokens_hbm, mixed, load_sems.at[3])
    token_load.start()
    lax.fori_loop(0, half - 1, greet, 0)

    @pl.when(is_inner)
    def _():
        pl.semaphore_signal(barrier, inc=1, device_id={"ep": far_dev})

    token_load.wait()
    for load in loads:
        load.start()

    def norm(i, carry):
        at = pl.ds(pl.multiple_of(i * 64, 64), 64)
        floats = mixed[at, :].astype(jnp.float32)
        scale = lax.rsqrt(jnp.mean(floats * floats, axis=-1, keepdims=True) + EPS)
        value = (floats * scale * gain[...]).astype(jnp.bfloat16)
        for c in range(chunks):
            normed[c, at, :] = value[:, c * step : (c + 1) * step]
        return carry

    lax.fori_loop(0, rows // 64, norm, 0)

    @pl.when(is_inner)
    def _():
        pl.semaphore_wait(barrier, half)

    @pl.when(is_outer)
    def _():
        pl.semaphore_wait(barrier, half - 1)

    def remote(src, dst, send, recv, device):
        return pltpu.make_async_remote_copy(
            src_ref=src, dst_ref=dst, send_sem=send, recv_sem=recv, device_id={"ep": device}
        )

    def span(j):
        return pl.ds(pl.multiple_of(j * capacity, 16), capacity)

    def table_to(k, source, device):
        return remote(source, tables.at[k], table_send.at[k], table_recv.at[k], device)

    def near_copy(c):
        return remote(normed.at[c], near.at[c], near_send.at[c], near_recv.at[c], inner_dev)

    def fin_copy(c):
        return remote(normed.at[c], far_in.at[c], fin_send.at[c], fin_recv.at[c], far_dev)

    def fout_copy(c):
        return remote(near.at[c], far_out.at[c], fout_send.at[c], fout_recv.at[c], far_dev)

    def own_sum(c):
        return remote(far_in.at[c], sum_own.at[c], own_send.at[c], own_recv.at[c], far_dev)

    def near_sum(c):
        return remote(far_out.at[c], sum_near.at[c], rel_send.at[c], rel_recv.at[c], far_dev)

    def up_copy(c):
        return remote(near.at[c], near.at[c], up_send.at[c], up_recv.at[c], outer_dev)

    def go_copy(k, c, peer, slot):
        return remote(
            packed.at[max(k - 1, 0), c, span(peer)], arrived.at[k, c, span(p)],
            go_send.at[max(k - 1, 0), c, slot], go_recv.at[k, c, p], base + peer,
        )

    def goo_copy(c, other, slot):
        return remote(
            packed_o.at[c, span(other)], arrived.at[1, c, span(p)],
            goo_send.at[c, slot], go_recv.at[1, c, p], plane + other,
        )

    def arrival(k, c, other, device):
        return remote(
            packed_o.at[c, span(other)], arrived.at[k, c, span(other)],
            goo_send.at[c, 0], go_recv.at[k, c, other], device,
        )

    def back_copy(k, c, other, slot):
        if k == 1:
            return remote(
                arrived.at[1, c, span(other)], backs_o.at[c, span(p)],
                back_send.at[1, c, slot], backo_recv.at[c, p], plane + other,
            )
        return remote(
            arrived.at[k, c, span(other)], backs.at[max(k - 1, 0), c, span(q)],
            back_send.at[k, c, slot], back_recv.at[max(k - 1, 0), c, q], inner_plane + other,
        )

    def back_arrival(k, c, peer):
        return remote(
            arrived.at[k, c, span(0)], backs.at[max(k - 1, 0), c, span(peer)],
            back_send.at[k, c, 0], back_recv.at[max(k - 1, 0), c, peer], base + peer,
        )

    def backo_arrival(c, other):
        return remote(
            arrived.at[1, c, span(0)], backs_o.at[c, span(other)],
            back_send.at[1, c, 0], backo_recv.at[c, other], plane + other,
        )

    def go_self(k, c):
        src = packed_o.at[c, span(p)] if k == 1 else packed.at[max(k - 1, 0), c, span(q)]
        return pltpu.make_async_copy(src, arrived.at[k, c, span(p)], self_go.at[k, c])

    def back_self(k, c):
        dst = backs_o.at[c, span(p)] if k == 1 else backs.at[max(k - 1, 0), c, span(q)]
        return pltpu.make_async_copy(arrived.at[k, c, span(p)], dst, self_back.at[k, c])

    def loop(number, act):
        def one(i, carry):
            act(i)
            return carry

        lax.fori_loop(0, number, one, 0)

    def each_peer(act):
        loop(half - 1, lambda i: act(peer_at(i), i))

    def each_near(act):
        loop(quarter - 1, lambda i: act((p + 1 + i) % quarter, i))

    def each_all(act):
        loop(quarter, lambda i: act((p + i) % quarter, i))

    def matrices(k, source, first, number):
        lanes = 128

        def one(i):
            at = pl.multiple_of(i * lanes, lanes)
            slots = (first + at + lax.broadcasted_iota(jnp.int32, (lanes, rows), 0)).astype(jnp.float32)
            taken = jnp.zeros((lanes, rows), jnp.float32)
            total = jnp.zeros((lanes, rows), jnp.float32)
            for t in range(top):
                hit = source[t : t + 1, :] == slots
                taken = taken + jnp.where(hit, 1.0, 0.0)
                total = total + jnp.where(hit, source[top + t : top + t + 1, :], 0.0)
            takes[k, pl.ds(at, lanes), :] = taken.astype(jnp.bfloat16)
            highs[k, :, pl.ds(at, lanes)] = total.T.astype(jnp.bfloat16)

        loop(number // lanes, one)

    def tiles(act):
        loop(step // TILE, lambda i: act(pl.ds(pl.multiple_of(i * TILE, TILE), TILE)))

    def pack(k, c, source):
        def one(cols):
            packed[max(k - 1, 0), c, :, cols] = dot32(takes[k], source[c, :, cols]).astype(jnp.bfloat16)

        tiles(one)
        each_peer(lambda peer, i: go_copy(k, c, peer, i).start())
        go_self(k, c).start()

    def pack_o(c, source):
        def one(cols):
            packed_o[c, :, cols] = dot32(takes[1, : count // 2], source[c, :, cols]).astype(jnp.bfloat16)

        tiles(one)
        each_near(lambda other, i: goo_copy(c, other, i).start())
        go_self(1, c).start()

    def expert(k, inner):
        for c in range(chunks):
            if k == 1:
                each_near(lambda other, i: arrival(1, c, other, plane + other).wait_recv())
            elif inner:
                each_near(lambda other, i: arrival(k, c, other, inner_plane + other).wait_recv())
            else:
                each_all(lambda other, i: arrival(k, c, other, inner_plane + other).wait_recv())
            if inner or k == 1:
                go_self(k, c).wait()

        def one(i):
            cols = pl.ds(pl.multiple_of(i * TILE, TILE), TILE)
            gate_pre = dot32(arrived[k, 0], w_gate[0:step, cols])
            up_pre = dot32(arrived[k, 0], w_up[0:step, cols])
            for c in range(1, chunks):
                gate_pre += dot32(arrived[k, c], w_gate[c * step : (c + 1) * step, cols])
                up_pre += dot32(arrived[k, c], w_up[c * step : (c + 1) * step, cols])
            hidden[:, cols] = (gate_pre / (1.0 + jnp.exp(-gate_pre)) * up_pre).astype(jnp.bfloat16)

        loop(ff // TILE, one)
        for c in range(chunks):

            def out(i):
                at = pl.multiple_of(i * TILE, TILE)
                cols = pl.ds(pl.multiple_of(c * step + at, TILE), TILE)
                arrived[k, c, :, pl.ds(at, TILE)] = dot32(hidden[...], w_down[:, cols]).astype(jnp.bfloat16)

            loop(step // TILE, out)
            if inner or k == 1:
                each_near(lambda other, i: back_copy(k, c, other, i).start())
                back_self(k, c).start()
            else:
                each_all(lambda other, i: back_copy(k, c, other, i).start())

    def wait_back(k, c):
        each_peer(lambda peer, i: back_arrival(k, c, peer).wait_recv())
        back_self(k, c).wait()

    def wait_backo(c):
        each_near(lambda other, i: backo_arrival(c, other).wait_recv())
        back_self(1, c).wait()

    def combine(k, c, cols):
        return dot32(highs[k], backs[max(k - 1, 0), c, :, cols])

    def combine_o(c, cols):
        return dot32(highs[1, :, : count // 2], backs_o[c, :, cols])

    def out_cols(c, i):
        return pl.ds(pl.multiple_of(c * step + i * TILE, TILE), TILE)

    def in_cols(i):
        return pl.ds(pl.multiple_of(i * TILE, TILE), TILE)

    def wait_loads():
        for load in loads:
            load.wait()

    @pl.when(is_inner)
    def _():
        first = base * capacity
        table_to(2, table, far_dev).start()
        fin_copy(0).start()
        fin_copy(1).start()
        matrices(0, table, first, count)
        for c in range(chunks):
            pack(0, c, normed)
        table_to(1, table, inner_dev).wait_recv()
        table_to(3, tables.at[1], far_dev).start()
        matrices(1, tables.at[1], plane * capacity, count // 2)
        table_to(2, table, far_dev).wait_recv()
        matrices(2, tables.at[2], first, count)

        def relay(c):
            near_copy(c).wait_recv()
            fout_copy(c).start()
            pack_o(c, near)

        def take_in(c):
            fin_copy(c).wait_recv()
            pack(2, c, far_in)

        def take_out(c):
            fout_copy(c).wait_recv()
            pack(3, c, far_out)

        relay(0)
        take_in(0)
        table_to(3, tables.at[1], far_dev).wait_recv()
        matrices(3, tables.at[3], first, count)
        relay(1)
        take_in(1)
        relay(2)
        take_out(0)
        relay(3)
        for c in range(2, chunks):
            fin_copy(c).start()
        wait_loads()
        take_out(1)
        expert(0, True)
        take_out(2)
        expert(1, True)
        take_out(3)
        for c in range(2, chunks):
            take_in(c)
        expert(3, True)
        expert(2, True)

        for c in range(chunks):
            wait_back(3, c)

            def merge_out(cols):
                far_out[c, :, cols] = combine(3, c, cols).astype(jnp.bfloat16)

            tiles(merge_out)
            near_sum(c).start()
        for c in range(chunks):
            wait_back(2, c)

            def merge_in(cols):
                far_in[c, :, cols] = combine(2, c, cols).astype(jnp.bfloat16)

            tiles(merge_in)
            own_sum(c).start()
            wait_backo(c)
            near_sum(c).wait_recv()
            fout_copy(c).wait_send()

            def rise(cols):
                total = combine_o(c, cols) + sum_near[c, :, cols].astype(jnp.float32)
                near[c, :, cols] = total.astype(jnp.bfloat16)

            tiles(rise)
            up_copy(c).start()
        for c in range(chunks):
            wait_back(0, c)
            own_sum(c).wait_recv()

            def close(i):
                total = combine(0, c, in_cols(i)) + sum_own[c, :, in_cols(i)].astype(jnp.float32)
                mixed[:, out_cols(c, i)] = total.astype(jnp.bfloat16)

            loop(step // TILE, close)
        table_to(2, table, far_dev).wait_send()
        table_to(3, tables.at[1], far_dev).wait_send()
        for c in range(chunks):
            fin_copy(c).wait_send()
            near_sum(c).wait_send()
            own_sum(c).wait_send()
            up_copy(c).wait_send()
            each_near(lambda other, i: goo_copy(c, other, i).wait_send())
            for k in (0, 2, 3):
                each_peer(lambda peer, i: go_copy(k, c, peer, i).wait_send())
            for k in range(4):
                each_near(lambda other, i: back_copy(k, c, other, i).wait_send())

    @pl.when(is_outer)
    def _():
        table_to(1, table, inner_dev).start()
        for c in range(chunks):
            near_copy(c).start()
        matrices(1, table, plane * capacity, count // 2)
        for c in range(chunks):
            pack_o(c, normed)
        wait_loads()
        expert(1, False)
        expert(0, False)
        expert(3, False)
        expert(2, False)
        for c in range(chunks):
            wait_backo(c)
            up_copy(c).wait_recv()

            def close(i):
                total = combine_o(c, in_cols(i)) + near[c, :, in_cols(i)].astype(jnp.float32)
                mixed[:, out_cols(c, i)] = total.astype(jnp.bfloat16)

            loop(step // TILE, close)
        table_to(1, table, inner_dev).wait_send()
        for c in range(chunks):
            near_copy(c).wait_send()
            each_near(lambda other, i: goo_copy(c, other, i).wait_send())
            each_near(lambda other, i: back_copy(1, c, other, i).wait_send())
            for k in (0, 2, 3):
                each_all(lambda other, i: back_copy(k, c, other, i).wait_send())


def body(tokens, norm_gain, route_ids, route_gates, w_gate, w_up, w_down):
    rows, width = tokens.shape
    top = route_ids.shape[1]
    devices = lax.axis_size("ep")
    experts = devices
    ff = w_gate.shape[2]
    capacity = 3 * rows * top // (2 * experts)
    half, quarter = devices // 2, devices // 4
    count = half * capacity
    step = width // CHUNKS
    weights = (route_gates / jnp.sum(route_gates, axis=1, keepdims=True)).T
    table = jnp.concatenate([slot_index(route_ids, experts, capacity), weights])
    vmem = pl.BlockSpec(memory_space=pltpu.VMEM)
    hbm = pl.BlockSpec(memory_space=pl.ANY)
    bf16 = jnp.bfloat16
    dma = pltpu.SemaphoreType.DMA
    block = (CHUNKS, rows, step)
    each = dma((CHUNKS,))
    return pl.pallas_call(
        functools.partial(kernel, devices, capacity, top),
        out_shape=jax.ShapeDtypeStruct((rows, width), bf16),
        in_specs=[hbm, vmem, vmem, hbm, hbm, hbm],
        out_specs=vmem,
        scratch_shapes=[
            pltpu.VMEM(block, bf16),
            pltpu.VMEM(block, bf16),
            pltpu.VMEM(block, bf16),
            pltpu.VMEM(block, bf16),
            pltpu.VMEM((4,) + table.shape, jnp.float32),
            pltpu.VMEM((4, count, rows), bf16),
            pltpu.VMEM((4, rows, count), bf16),
            pltpu.VMEM((3, CHUNKS, count, step), bf16),
            pltpu.VMEM((CHUNKS, count // 2, step), bf16),
            pltpu.VMEM((4, CHUNKS, count // 2, step), bf16),
            pltpu.VMEM((count // 2, ff), bf16),
            pltpu.VMEM((width, ff), bf16),
            pltpu.VMEM((width, ff), bf16),
            pltpu.VMEM((ff, width), bf16),
            pltpu.VMEM((3, CHUNKS, count, step), bf16),
            pltpu.VMEM((CHUNKS, count // 2, step), bf16),
            pltpu.VMEM(block, bf16),
            pltpu.VMEM(block, bf16),
            dma((4,)), dma((4,)), dma((4,)),
            each, each, each, each, each, each,
            dma((3, CHUNKS, half)),
            dma((4, CHUNKS, quarter)),
            dma((CHUNKS, quarter)),
            dma((4, CHUNKS, quarter)),
            dma((3, CHUNKS, half)),
            dma((CHUNKS, quarter)),
            dma((4, CHUNKS)),
            dma((4, CHUNKS)),
            each, each, each, each, each, each,
        ],
        compiler_params=pltpu.CompilerParams(
            collective_id=0, has_side_effects=True, vmem_limit_bytes=VMEM_BYTES
        ),
    )(tokens, norm_gain[None, :], table, w_gate, w_up, w_down)


def solution(mesh):
    placed = (
        P(("grp", "ep"), None),
        P(),
        P(("grp", "ep"), None),
        P(("grp", "ep"), None),
        P("ep", None, None),
        P("ep", None, None),
        P("ep", None, None),
    )
    return jax.shard_map(
        body, mesh=mesh, in_specs=placed, out_specs=P(("grp", "ep"), None), check_vma=False
    )
```

time: 382 us -> 274 us (0.72)
  Pallas kernels: 0 us -> 266 us
  blocking collectives: 144 us -> 0 us
  waiting for transfers between devices: 137 us -> 0 us
  local copies, waits for them, and re-layouts: 46.1 us -> 3.93 us
  other arithmetic: 25.1 us -> 2.02 us
  matrix products: 23.2 us -> 0.26 us
  starting transfers between devices: 5.55 us -> 0 us
    pallas_call x0 -> x1, Pallas kernels: none -> 266 us  [body(): pl.pallas_call(functools.partial(kernel, devices, capacity, top), out_sha...]
    all_to_all x1 -> x0, blocking collectives: 144 us -> none  [body(): lax.all_to_all(outgoing, 'ep', split_axis=0, concat_axis=0, tiled=True)]
    all_to_all x1 -> x0, waiting for transfers between devices: 137 us -> none  [body(): lax.all_to_all(finished, 'ep', split_axis=0, concat_axis=0, tiled=True)]
    dot_general x3 -> x1, matrix products: 23.2 us -> 0.26 us  [slot_index(): jnp.dot(before, named.astype(jnp.bfloat16), preferred_element_type=jnp.fl...]
    scatter x1 -> x0, local copies, waits for them, and re-layouts: 22 us -> none  [body(): jnp.zeros((experts * capacity, width), jnp.bfloat16).at[places]]
    reduce_sum x4 -> x1, other arithmetic: 17.1 us -> 0.7 us  [body(): weights = (route_gates / jnp.sum(route_gates, axis=1, keepdims=True)).T]
    gather x1 -> x0, local copies, waits for them, and re-layouts: 12.4 us -> none  [body(): picked = returned.reshape(experts * capacity, width)[places]]
    convert_element_type x1 -> x0, local copies, waits for them, and re-layouts: 9.65 us -> none  [body(): shaped = picked.astype(jnp.float32).reshape(tok_rows, top_count, width)]
  transfers between devices with their start and end apart: 1 -> 0, of which waited for: 1 -> 0; matrix products, arithmetic and copies ran while one was open for 0% -> 0% of each run, Pallas kernels for 0% -> 0%
where the time goes in v3:
time: 274 us; the launch traced here: 273 us
  Pallas kernels  266 us (97%)
  local copies, waits for them, and re-layouts  3.93 us (1%)
    pallas_call x1, Pallas kernels, body(): pl.pallas_call(functools.partial(kernel, devices, capacity, top), out_sha...  266 us

profile of v3, /device:TPU:15, one launch (start us, length us, event | category | flops | bytes accessed | tf_op | source)
XLA Modules:
  0.0 272.7 jit_solution(5307007430429889571)
XLA Ops:
  0.0 0.7 reduce_sum.29
  0.7 0.7 divide_bitcast_fusion
  1.4 0.8 fusion.2
  2.2 0.3 select_reduce_fusion.1
  2.4 0.6 pad_maximum_fusion.table
  3.1 266.5 %shard_map.73 = bf16[512,2048]{1,0:T(8,128)(2,1)} custom-call(bf16[512,2048]{1,0:T(8,128)(2,1)} %tokens_hbm.1, f32[1,2048]{1,0:T(1,128)} %bitcast.7, f32[4,512]{1,0:T(4,128)} %pad_maximum_fusion.table, bf16[1,2048,1024]{2,1,0:T(8,128)(2,1)} %gate_hbm.1, bf16[1,2048,1024]{2,1,0:T(8,128)(2,1)} %up_hbm.1, bf16[1,1024,2048]{2,1,0:T(8,128)(2,1)} %down_hbm.1), custom_call_target="tpu_custom_call" | custom-call | tf_op jit(solution)/shard_map/pallas_call | solution.py:441
  269.6 3.2 %copy.9 = bf16[512,2048]{1,0:T(8,128)(2,1)} copy(bf16[512,2048]{1,0:T(8,128)(2,1)} %shard_map.73) | data formatting | bytes 4194304
  (1 shorter events, 0.0 us)

commit v4 on v2

--- a/solution.py
+++ b/solution.py
@@ -11,12 +11,6 @@
 CHUNKS = 4
 TILE = 256
 VMEM_BYTES = 66000000
-
-
-def rms_norm(tokens, norm_gain):
-    floats = tokens.astype(jnp.float32)
-    scale = lax.rsqrt(jnp.mean(floats * floats, axis=-1, keepdims=True) + EPS)
-    return (floats * scale * norm_gain).astype(jnp.bfloat16)
 
 
 def slot_index(route_ids, experts, capacity):
@@ -35,9 +29,9 @@
 
 def kernel(
     devices, capacity, top,
-    normed, table, gate_hbm, up_hbm, down_hbm,
+    tokens_hbm, gain, table, gate_hbm, up_hbm, down_hbm,
     mixed,
-    far, far_table, takes, highs, lows, packed, arrived, hidden, w_gate, w_up, w_down,
+    normed, far, far_table, takes, highs, lows, packed, arrived, hidden, w_gate, w_up, w_down,
     outs, backs, partial, partial_in,
     weight_sems, table_sems, far_send, far_recv, own_sems, self_sems, go_send, go_recv,
     back_send, back_recv, part_send, part_recv,
@@ -62,6 +56,8 @@
         pl.semaphore_signal(barrier, inc=1, device_id={"ep": base + peer_at(i)})
         return carry
 
+    token_load = pltpu.make_async_copy(tokens_hbm, mixed, weight_sems.at[3])
+    token_load.start()
     lax.fori_loop(0, half - 1, greet, 0)
     pl.semaphore_signal(barrier, inc=1, device_id={"ep": partner})
 
@@ -70,6 +66,18 @@
         pltpu.make_async_copy(up_hbm.at[0], w_up, weight_sems.at[1]),
         pltpu.make_async_copy(down_hbm.at[0], w_down, weight_sems.at[2]),
     ]
+    token_load.wait()
+
+    def norm(i, carry):
+        at = pl.ds(pl.multiple_of(i * 64, 64), 64)
+        floats = mixed[at, :].astype(jnp.float32)
+        scale = lax.rsqrt(jnp.mean(floats * floats, axis=-1, keepdims=True) + EPS)
+        value = (floats * scale * gain[...]).astype(jnp.bfloat16)
+        for c in range(chunks):
+            normed[c, at, :] = value[:, c * step : (c + 1) * step]
+        return carry
+
+    lax.fori_loop(0, rows // 64, norm, 0)
     pl.semaphore_wait(barrier, half)
 
     def remote(src, dst, send, recv, device):
@@ -220,6 +228,8 @@
                 expert_out(0, d)
     for c in range(chunks):
         wait_go(1, c)
+    for c in range(1):
+        send_back(0, c)
     expert_hidden(1)
     for c in range(chunks):
         expert_out(1, c)
@@ -233,7 +243,8 @@
 
         tiles(merge)
         part_copy(c).start()
-        send_back(0, c)
+        if c >= 1:
+            send_back(0, c)
     for c in range(chunks):
         wait_back(0, c)
         part_copy(c).wait_recv()
@@ -265,7 +276,6 @@
     half = devices // 2
     count = half * capacity
     step = width // CHUNKS
-    normed = rms_norm(tokens, norm_gain).reshape(rows, CHUNKS, step).transpose(1, 0, 2)
     weights = (route_gates / jnp.sum(route_gates, axis=1, keepdims=True)).T
     table = jnp.concatenate([slot_index(route_ids, experts, capacity), weights])
     vmem = pl.BlockSpec(memory_space=pltpu.VMEM)
@@ -275,9 +285,10 @@
     return pl.pallas_call(
         functools.partial(kernel, devices, capacity, top),
         out_shape=jax.ShapeDtypeStruct((rows, width), bf16),
-        in_specs=[vmem, vmem, hbm, hbm, hbm],
+        in_specs=[hbm, vmem, vmem, hbm, hbm, hbm],
         out_specs=vmem,
         scratch_shapes=[
+            pltpu.VMEM((CHUNKS, rows, step), bf16),
             pltpu.VMEM((CHUNKS, rows, step), bf16),
             pltpu.VMEM(table.shape, jnp.float32),
             pltpu.VMEM((2, count, rows), bf16),
@@ -293,7 +304,7 @@
             pltpu.VMEM((2, CHUNKS, count, step), bf16),
             pltpu.VMEM((CHUNKS, rows, step), bf16),
             pltpu.VMEM((CHUNKS, rows, step), bf16),
-            dma((3,)),
+            dma((4,)),
             dma((2,)),
             dma((CHUNKS,)),
             dma((CHUNKS,)),
@@ -309,7 +320,7 @@
         compiler_params=pltpu.CompilerParams(
             collective_id=0, has_side_effects=True, vmem_limit_bytes=VMEM_BYTES
         ),
-    )(normed, table, w_gate, w_up, w_down)
+    )(tokens, norm_gain[None, :], table, w_gate, w_up, w_down)
 
 
 def solution(mesh):

time: 265 us -> 248 us (0.936)
  Pallas kernels: 249 us -> 239 us
  local copies, waits for them, and re-layouts: 10.9 us -> 3.93 us
    pallas_call x1, Pallas kernels: 249 us -> 239 us  [body(): pl.pallas_call(functools.partial(kernel, devices, capacity, top), out_sha...]
    reshape x1 -> x0, local copies, waits for them, and re-layouts: 4.14 us -> none  [body(): rms_norm(tokens, norm_gain).reshape(rows, CHUNKS, step).transpose(1, 0, 2)]
    unnamed x4 -> x1, local copies, waits for them, and re-layouts: 6.02 us -> 3.16 us
where the time goes in v4:
time: 248 us; the launch traced here: 245 us
  Pallas kernels  239 us (96%)
  local copies, waits for them, and re-layouts  3.93 us (2%)
    pallas_call x1, Pallas kernels, body(): pl.pallas_call(functools.partial(kernel, devices, capacity, top), out_sha...  239 us

profile of v4, /device:TPU:15, one launch (start us, length us, event | category | flops | bytes accessed | tf_op | source)
XLA Modules:
  0.0 245.5 jit_solution(16343209545891360338)
XLA Ops:
  0.0 0.7 reduce_sum.29
  0.7 0.7 divide_bitcast_fusion
  1.4 0.8 fusion.2
  2.2 0.3 select_reduce_fusion.1
  2.4 0.6 pad_maximum_fusion.table
  3.1 239.2 %shard_map.73 = bf16[512,2048]{1,0:T(8,128)(2,1)} custom-call(bf16[512,2048]{1,0:T(8,128)(2,1)} %tokens_hbm.1, f32[1,2048]{1,0:T(1,128)} %bitcast.7, f32[4,512]{1,0:T(4,128)} %pad_maximum_fusion.table, bf16[1,2048,1024]{2,1,0:T(8,128)(2,1)} %gate_hbm.1, bf16[1,2048,1024]{2,1,0:T(8,128)(2,1)} %up_hbm.1, bf16[1,1024,2048]{2,1,0:T(8,128)(2,1)} %down_hbm.1), custom_call_target="tpu_custom_call" | custom-call | tf_op jit(solution)/shard_map/pallas_call | solution.py:285
  242.3 3.2 %copy.9 = bf16[512,2048]{1,0:T(8,128)(2,1)} copy(bf16[512,2048]{1,0:T(8,128)(2,1)} %shard_map.73) | data formatting | bytes 4194304
  (1 shorter events, 0.0 us)
